TPU v7x, 32 devices: a whole 2x2x4 slice. The times are simulated.
32 devices in a mesh: ra: 4 (over z), cb: 4 (over y, x), dp: 2 (over core).
Axes of the slice: x: 2, y: 2, z: 4, core: 2. Of those that a mesh axis runs over, the one named last changes fastest.
Arguments:
- tokens: bfloat16 [2048, 4096], P('dp', 'cb'), may hold values from -3000 to 3000
- norm_gain: float32 [4096], P('cb'), may hold values from 0.1 to 1.9
- norm_bias: float32 [4096], P('cb'), may hold values from -2 to 2
- gate_weight: float32 [4096, 11264], P('cb', 'ra'), may hold values from -0.09375 to 0.09375
- up_weight: float32 [4096, 11264], P('cb', 'ra'), may hold values from -0.09375 to 0.09375
- gate_scale: float32 [11264], P('ra'), may hold values from 0.5 to 2
- up_scale: float32 [11264], P('ra'), may hold values from 0.5 to 2
- down_weight: float32 [11264, 4096], P('ra', 'cb'), may hold values from -0.0546875 to 0.0546875
- down_scale: float32 [4096], P('cb'), may hold values from 0.5 to 8
- out_gain: float32 [4096], P('cb'), may hold values from 0.1 to 1.9
- out_bias: float32 [4096], P('cb'), may hold values from -2 to 2
Outputs:
- result: bfloat16 [2048, 4096], P(('dp', 'ra'), 'cb')
All inputs are finite; a program needn't handle non-finite values.
Results may differ from a plain program's by a relative error of at most 0.018.
Values may be sent and summed in bfloat16 or wider, within the bound.
A program may use at most 128 MiB of HBM per device.

v0:
```python
import jax
import jax.numpy as jnp
from jax import lax
from jax.experimental import pallas as pl
from jax.experimental.pallas import tpu as pltpu
from jax.sharding import PartitionSpec as P

MESH = pl.DeviceIdType.MESH
EPS = 1e-05
TILE = 256
G = 4
F32 = jnp.float32
BF16 = jnp.bfloat16


def standardize(values):
    width = values.shape[1] * lax.axis_size("cb")
    total = lax.psum(jnp.sum(values, axis=1), "cb")
    mean = total / width
    centred = values - mean[:, None]
    spread = lax.psum(jnp.sum(centred * centred, axis=1), "cb") / width
    return centred * lax.rsqrt(spread + EPS)[:, None]


def plain(
    tokens,
    norm_gain,
    norm_bias,
    gate_weight,
    up_weight,
    gate_scale,
    up_scale,
    down_weight,
    down_scale,
    out_gain,
    out_bias,
):
    normed = (standardize(tokens.astype(F32)) * norm_gain + norm_bias).astype(BF16)
    gate_part = jnp.dot(normed, gate_weight.astype(BF16), preferred_element_type=F32)
    up_part = jnp.dot(normed, up_weight.astype(BF16), preferred_element_type=F32)
    gate_share, up_share = (
        lax.psum_scatter(part.astype(BF16), "cb", scatter_dimension=1, tiled=True).astype(F32)
        for part in (gate_part, up_part)
    )
    share = gate_share.shape[1]
    offset = lax.axis_index("cb") * share
    gate_cols = lax.dynamic_slice_in_dim(gate_scale, offset, share, 0)
    up_cols = lax.dynamic_slice_in_dim(up_scale, offset, share, 0)
    hidden_share = (jax.nn.silu(gate_share * gate_cols) * (up_share * up_cols)).astype(BF16)
    hidden = lax.all_gather(hidden_share, "cb", axis=1, tiled=True)
    own_rows = hidden.shape[0] // lax.axis_size("ra")
    part = jnp.dot(hidden, down_weight.astype(BF16), preferred_element_type=F32)
    branch = lax.psum_scatter(part, "ra", scatter_dimension=0, tiled=True) * down_scale
    own_normed = lax.dynamic_slice_in_dim(normed, lax.axis_index("ra") * own_rows, own_rows, 0)
    mixed = 0.5 * own_normed.astype(F32) + branch
    return (standardize(mixed) * out_gain + out_bias).astype(BF16)


NC = 8
SKEW = (0, 1, 2, 3, 4)


def schedule():
    steps = []
    for t in range(NC + max(SKEW)):
        for stage, behind in enumerate(SKEW):
            if 0 <= t - behind < NC:
                steps.append((stage, t - behind))
    return steps


def kernel(
    tok,
    ng,
    nb,
    gw,
    uw,
    gs,
    us,
    dw,
    down_scale,
    og,
    ob,
    out,
    stage,
    stage_d,
    wg,
    wu,
    wd,
    nrm,
    pg,
    pu,
    r1g,
    r1u,
    rdg,
    r2g,
    rdu,
    r2u,
    hid,
    bp,
    zr,
    mix,
    st,
    st2,
    stage_sem,
    stage_d_sem,
    send,
    recv,
    st_send,
    st_recv,
):
    rows, width = tok.shape
    ff = wg.shape[1]
    tiles = ff // TILE
    blk = rows // (G * NC)
    chunk = G * blk
    part = rows // G
    full = float(width * G)

    b = lax.axis_index("cb")
    r = lax.axis_index("ra")
    xn = b + 1 - 2 * lax.rem(b, 2)
    yn = lax.rem(b + 2, G)
    dg = (G - 1) - b
    zs = [lax.rem(r + o, G) for o in range(1, G)]

    def to(axis, index):
        return {axis: index}

    peers = [to("cb", xn), to("cb", yn), to("cb", dg)] + [to("ra", z) for z in zs]
    barrier = pltpu.get_barrier_semaphore()
    for peer in peers:
        pl.semaphore_signal(barrier, inc=1, device_id=peer, device_id_type=MESH)

    def tile_cols(t):
        return pl.ds(pl.multiple_of(t * TILE, TILE), TILE)

    def load_gu(t, slot):
        return (
            pltpu.make_async_copy(gw.at[:, tile_cols(t)], stage.at[slot], stage_sem.at[slot]),
            pltpu.make_async_copy(uw.at[:, tile_cols(t)], stage.at[2 + slot], stage_sem.at[2 + slot]),
        )

    for t in range(2):
        for copy in load_gu(t, t):
            copy.start()

    def put_stats(x, dst, col):
        total = jnp.sum(x, axis=1, keepdims=True)
        off = x - total * (1.0 / width)
        spread = jnp.sum(off * off, axis=1, keepdims=True)
        lane = lax.broadcasted_iota(jnp.int32, (x.shape[0], 128), 1)
        both = jnp.where(lane == 0, total, spread)
        dst[0, :, pl.ds(col, x.shape[0])] = both.T[:8, :]

    def get_stats(src, col, n):
        parts = [src[i, 0:2, pl.ds(col, n)] for i in range(G)]
        mean = (parts[0][0:1] + parts[1][0:1] + parts[2][0:1] + parts[3][0:1]) / full
        spread = jnp.zeros_like(mean)
        for p in parts:
            d = p[0:1] * (1.0 / width) - mean
            spread = spread + p[1:2] + width * (d * d)
        inv = lax.rsqrt(spread / full + EPS)
        sub = lax.broadcasted_iota(jnp.int32, (128, n), 0)
        both = jnp.where(sub == 0, mean, inv).T
        return both[:, 0:1], both[:, 1:2]

    def swap_stats(buf, which):
        copies = []
        for i, peer in enumerate(peers[:3]):
            copies.append(
                pltpu.make_async_remote_copy(
                    src_ref=buf.at[0],
                    dst_ref=buf.at[1 + i],
                    send_sem=st_send.at[which, i],
                    recv_sem=st_recv.at[which, i],
                    device_id=peer,
                    device_id_type=MESH,
                )
            )
        return copies

    for j in range(G):
        put_stats(tok[pl.ds(j * part, part), :].astype(F32), st, j * part)

    pl.semaphore_wait(barrier, len(peers))
    swap1 = swap_stats(st, 0)
    for copy in swap1:
        copy.start()

    def cast_gu(t, carry):
        slot = lax.rem(t, 2)
        for copy in load_gu(t, slot):
            copy.wait()
        wg[:, tile_cols(t)] = stage[slot].astype(BF16)
        wu[:, tile_cols(t)] = stage[2 + slot].astype(BF16)

        @pl.when(t + 2 < tiles)
        def _():
            for copy in load_gu(t + 2, slot):
                copy.start()

        return carry

    lax.fori_loop(0, tiles, cast_gu, 0)

    def tile_rows(t):
        return pl.ds(pl.multiple_of(t * TILE, TILE), TILE)

    def load_d(t, slot):
        return pltpu.make_async_copy(dw.at[tile_rows(t), :], stage_d.at[slot], stage_d_sem.at[slot])

    for t in range(2):
        load_d(t, t).start()

    for copy in swap1:
        copy.wait_recv()
    for j in range(G):
        mean, inv = get_stats(st, j * part, part)
        x = tok[pl.ds(j * part, part), :].astype(F32)
        y = ((x - mean) * inv * ng[...] + nb[...]).astype(BF16)
        for c in range(NC):
            nrm[c, pl.ds(j * blk, blk), :] = y[c * blk : (c + 1) * blk, :]

    def remote(kind, c, src, dst, peer):
        return pltpu.make_async_remote_copy(
            src_ref=src,
            dst_ref=dst,
            send_sem=send.at[kind, c],
            recv_sem=recv.at[kind, c],
            device_id=peer,
            device_id_type=MESH,
        )

    px, py = peers[0], peers[1]
    half = ff // 2 // 128 * 128
    cp = {}
    for c in range(NC):
        mine = pl.ds(pl.multiple_of(b * blk, blk), blk)
        of_x = pl.ds(pl.multiple_of(xn * blk, blk), blk)
        of_y = pl.ds(pl.multiple_of(yn * blk, blk), blk)
        lo, hi = pl.ds(0, half), pl.ds(half, ff - half)
        cp[c] = [
            remote(0, c, pg.at[c, dg], r1g.at[c], px),
            remote(1, c, pu.at[c, dg], r1u.at[c], py),
            remote(2, c, pg.at[c, xn], rdg.at[c], px),
            remote(3, c, pu.at[c, yn], rdu.at[c], py),
            remote(4, c, pg.at[c, yn], r2g.at[c], py),
            remote(5, c, pu.at[c, xn], r2u.at[c], px),
            remote(6, c, hid.at[c, mine], hid.at[c, mine], px),
            remote(7, c, hid.at[c, mine], hid.at[c, mine], py),
            remote(8, c, hid.at[c, of_x, lo], hid.at[c, of_x, lo], py),
            remote(9, c, hid.at[c, of_y, hi], hid.at[c, of_y, hi], px),
        ]
        for o, z in enumerate(zs):
            rowz = pl.ds(pl.multiple_of(z * blk, blk), blk)
            cp[c].append(remote(10 + o, c, bp.at[c, rowz], zr.at[c, o], peers[3 + o]))

    def s1(c):
        def body(t, carry):
            cols = tile_cols(t)
            x = nrm[c]
            g = jnp.dot(x, wg[:, cols], preferred_element_type=F32).astype(BF16)
            u = jnp.dot(x, wu[:, cols], preferred_element_type=F32).astype(BF16)
            for j in range(G):
                pg[c, j, :, cols] = g[j * blk : (j + 1) * blk, :]
                pu[c, j, :, cols] = u[j * blk : (j + 1) * blk, :]
            return carry

        lax.fori_loop(0, tiles, body, 0)
        for k in range(4):
            cp[c][k].start()

    def w_down(_):
        def body(t, carry):
            slot = lax.rem(t, 2)
            load_d(t, slot).wait()
            wd[tile_rows(t), :] = stage_d[slot].astype(BF16)

            @pl.when(t + 2 < tiles)
            def _():
                load_d(t + 2, slot).start()

            return carry

        lax.fori_loop(0, tiles, body, 0)

    def s2(c):
        cp[c][0].wait_recv()
        cp[c][1].wait_recv()

        def body(t, carry):
            cols = tile_cols(t)
            pg[c, yn, :, cols] = (pg[c, yn, :, cols].astype(F32) + r1g[c, :, cols].astype(F32)).astype(BF16)
            pu[c, xn, :, cols] = (pu[c, xn, :, cols].astype(F32) + r1u[c, :, cols].astype(F32)).astype(BF16)
            return carry

        lax.fori_loop(0, tiles, body, 0)
        cp[c][4].start()
        cp[c][5].start()

    def s3(c):
        for k in range(2, 6):
            cp[c][k].wait_recv()

        def body(t, carry):
            cols = tile_cols(t)
            g = pg[c, b, :, cols].astype(F32) + rdg[c, :, cols].astype(F32) + r2g[c, :, cols].astype(F32)
            u = pu[c, b, :, cols].astype(F32) + rdu[c, :, cols].astype(F32) + r2u[c, :, cols].astype(F32)
            g = g * gs[:, cols]
            u = u * us[:, cols]
            h = (g / (1.0 + jnp.exp(-g)) * u).astype(BF16)
            hid[c, pl.ds(pl.multiple_of(b * blk, blk), blk), cols] = h
            return carry

        lax.fori_loop(0, tiles, body, 0)
        cp[c][6].start()
        cp[c][7].start()

    def s4(c):
        cp[c][6].wait_recv()
        cp[c][8].start()
        cp[c][7].wait_recv()
        cp[c][9].start()

    def s5(c):
        cp[c][8].wait_recv()
        cp[c][9].wait_recv()

        def body(t, carry):
            cols = tile_cols(t)
            bp[c, :, cols] = jnp.dot(hid[c], wd[:, cols], preferred_element_type=F32).astype(BF16)
            return carry

        lax.fori_loop(0, width // TILE, body, 0)
        for o in (1, 0, 2):
            cp[c][10 + o].start()

    steps = (s1, s2, s3, s4, s5)
    for i, (step, c) in enumerate(schedule()):
        if i == 2:
            w_down(0)
        steps[step](c)

    mine = pl.ds(pl.multiple_of(r * blk, blk), blk)
    for c in range(NC):
        for o in (1, 0, 2):
            cp[c][10 + o].wait_recv()
        total = bp[c, mine, :].astype(F32)
        for o in range(G - 1):
            total = total + zr[c, o].astype(F32)
        mix[pl.ds(c * blk, blk), :] = 0.5 * nrm[c, mine, :].astype(F32) + total * down_scale[...]
    put_stats(mix[...], st2, 0)
    swap2 = swap_stats(st2, 1)
    for copy in swap2:
        copy.start()
    for copy in swap2:
        copy.wait_recv()
    mean, inv = get_stats(st2, 0, part)
    out[...] = ((mix[...] - mean) * inv * og[...] + ob[...]).astype(BF16)

    for copy in swap1 + swap2:
        copy.wait_send()
    for c in range(NC):
        for copy in cp[c]:
            copy.wait_send()


def fused(
    tokens,
    norm_gain,
    norm_bias,
    gate_weight,
    up_weight,
    gate_scale,
    up_scale,
    down_weight,
    down_scale,
    out_gain,
    out_bias,
):
    rows, width = tokens.shape
    ff = gate_weight.shape[1]
    blk = rows // (G * NC)
    chunk = G * blk
    part = rows // G
    vmem = pl.BlockSpec(memory_space=pltpu.VMEM)
    hbm = pl.BlockSpec(memory_space=pl.ANY)
    block = pltpu.VMEM((NC, blk, ff), BF16)
    row = lambda v: v.reshape(1, -1)
    return pl.pallas_call(
        kernel,
        out_shape=jax.ShapeDtypeStruct((part, width), BF16),
        in_specs=[vmem, vmem, vmem, hbm, hbm, vmem, vmem, hbm, vmem, vmem, vmem],
        out_specs=vmem,
        scratch_shapes=[
            pltpu.VMEM((4, width, TILE), F32),
            pltpu.VMEM((2, TILE, width), F32),
            pltpu.VMEM((width, ff), BF16),
            pltpu.VMEM((width, ff), BF16),
            pltpu.VMEM((ff, width), BF16),
            pltpu.VMEM((NC, chunk, width), BF16),
            pltpu.VMEM((NC, G, blk, ff), BF16),
            pltpu.VMEM((NC, G, blk, ff), BF16),
            block,
            block,
            block,
            block,
            block,
            block,
            pltpu.VMEM((NC, chunk, ff), BF16),
            pltpu.VMEM((NC, chunk, width), BF16),
            pltpu.VMEM((NC, G - 1, blk, width), BF16),
            pltpu.VMEM((part, width), F32),
            pltpu.VMEM((G, 8, rows), F32),
            pltpu.VMEM((G, 8, part), F32),
            pltpu.SemaphoreType.DMA((4,)),
            pltpu.SemaphoreType.DMA((2,)),
            pltpu.SemaphoreType.DMA((13, NC)),
            pltpu.SemaphoreType.DMA((13, NC)),
            pltpu.SemaphoreType.DMA((2, G - 1)),
            pltpu.SemaphoreType.DMA((2, G - 1)),
        ],
        compiler_params=pltpu.CompilerParams(
            collective_id=0, has_side_effects=True, vmem_limit_bytes=67043328
        ),
    )(
        tokens,
        row(norm_gain),
        row(norm_bias),
        gate_weight,
        up_weight,
        row(gate_scale),
        row(up_scale),
        down_weight,
        row(down_scale),
        row(out_gain),
        row(out_bias),
    )


def local(*args):
    rows, width = args[0].shape
    ff = args[3].shape[1]
    fits = (
        lax.axis_size("cb") == G
        and lax.axis_size("ra") == G
        and rows % (16 * G * NC) == 0
        and rows % (128 * G) == 0
        and width % TILE == 0
        and ff % TILE == 0
        and rows * width <= 1 << 20
        and ff * width <= 2816 * 1024
    )
    return (fused if fits else plain)(*args)


def solution(mesh):
    return jax.shard_map(
        local,
        mesh=mesh,
        in_specs=(
            P("dp", "cb"),
            P("cb"),
            P("cb"),
            P("cb", "ra"),
            P("cb", "ra"),
            P("ra"),
            P("ra"),
            P("ra", "cb"),
            P("cb"),
            P("cb"),
            P("cb"),
        ),
        out_specs=P(("dp", "ra"), "cb"),
        check_vma=False,
    )
```

profile of v0, /device:TPU:0, one launch (start us, length us, event | category | flops | bytes accessed | tf_op | source)
XLA Modules:
  0.0 183.7 jit_solution(8345732335909981805)
XLA Ops:
  0.0 1.3 reshape.23.gs
  1.3 1.3 reshape.24.us
  2.6 179.2 %shard_map.109 = bf16[256,1024]{1,0:T(8,128)(2,1)} custom-call(bf16[1024,1024]{1,0:T(8,128)(2,1)} %tok.1, f32[1,1024]{1,0:T(1,128)} %bitcast.5, f32[1,1024]{1,0:T(1,128)} %bitcast.6, f32[1024,2816]{1,0:T(8,128)} %gw.1, f32[1024,2816]{1,0:T(8,128)} %uw.1, f32[1,2816]{1,0:T(1,128)} %reshape.23.gs, f32[1,2816]{1,0:T(1,128)} %reshape.24.us, f32[2816,1024]{1,0:T(8,128)} %dw.1, ...), custom_call_target="tpu_custom_call" | custom-call | tf_op jit(solution)/shard_map/pallas_call | solution.py:391
  181.8 1.9 %copy.13 = bf16[256,1024]{1,0:T(8,128)(2,1)} copy(bf16[256,1024]{1,0:T(8,128)(2,1)} %shard_map.109) | data formatting | bytes 1048576
where the time goes:
time: 184 us
  Pallas kernels  179 us (97%)
  local copies, waits for them, and re-layouts  4.49 us (2%)
    pallas_call x1, Pallas kernels, fused(): pl.pallas_call(kernel, out_shape=jax.ShapeDtypeStruct((part, width), BF16...  179 us

commit v1 on v0

v1 whole, which is shorter than its diff:
```python
import jax
import jax.numpy as jnp
from jax import lax
from jax.experimental import pallas as pl
from jax.experimental.pallas import tpu as pltpu
from jax.sharding import PartitionSpec as P

MESH = pl.DeviceIdType.MESH
EPS = 1e-05
TILE = 256
LANE = 128
PIECES = 4
G = 4
F32 = jnp.float32
BF16 = jnp.bfloat16


def standardize(values):
    width = values.shape[1] * lax.axis_size("cb")
    total = lax.psum(jnp.sum(values, axis=1), "cb")
    mean = total / width
    centred = values - mean[:, None]
    spread = lax.psum(jnp.sum(centred * centred, axis=1), "cb") / width
    return centred * lax.rsqrt(spread + EPS)[:, None]


def plain(
    tokens,
    norm_gain,
    norm_bias,
    gate_weight,
    up_weight,
    gate_scale,
    up_scale,
    down_weight,
    down_scale,
    out_gain,
    out_bias,
):
    normed = (standardize(tokens.astype(F32)) * norm_gain + norm_bias).astype(BF16)
    gate_part = jnp.dot(normed, gate_weight.astype(BF16), preferred_element_type=F32)
    up_part = jnp.dot(normed, up_weight.astype(BF16), preferred_element_type=F32)
    gate_share, up_share = (
        lax.psum_scatter(part.astype(BF16), "cb", scatter_dimension=1, tiled=True).astype(F32)
        for part in (gate_part, up_part)
    )
    share = gate_share.shape[1]
    offset = lax.axis_index("cb") * share
    gate_cols = lax.dynamic_slice_in_dim(gate_scale, offset, share, 0)
    up_cols = lax.dynamic_slice_in_dim(up_scale, offset, share, 0)
    hidden_share = (jax.nn.silu(gate_share * gate_cols) * (up_share * up_cols)).astype(BF16)
    hidden = lax.all_gather(hidden_share, "cb", axis=1, tiled=True)
    own_rows = hidden.shape[0] // lax.axis_size("ra")
    part = jnp.dot(hidden, down_weight.astype(BF16), preferred_element_type=F32)
    branch = lax.psum_scatter(part, "ra", scatter_dimension=0, tiled=True) * down_scale
    own_normed = lax.dynamic_slice_in_dim(normed, lax.axis_index("ra") * own_rows, own_rows, 0)
    mixed = 0.5 * own_normed.astype(F32) + branch
    return (standardize(mixed) * out_gain + out_bias).astype(BF16)


def tiles_of(ff):
    wide = (ff // LANE + 3) // 4 * LANE
    narrow = ff // 2 - wide
    count = (wide + TILE - 1) // TILE
    both = []
    for t in range(count):
        off = t * TILE
        both.append(((off, min(TILE, wide - off)), (off, min(TILE, narrow - off))))
    return wide, narrow, both


def kernel(
    tok,
    ng,
    nb,
    gw,
    uw,
    gs,
    us,
    dw,
    down_scale,
    og,
    ob,
    out,
    stage,
    stage_d,
    wa,
    wb,
    sa,
    sb,
    xt,
    gb,
    la,
    lb,
    pa,
    pb,
    ca,
    cb,
    ra,
    rb,
    hid,
    wd,
    bp,
    zr,
    mix,
    ms,
    st,
    st2,
    stage_sem,
    stage_d_sem,
    tok_s,
    tok_r,
    z_s,
    z_r,
    gb_s,
    gb_r,
    w_s,
    w_r,
    f_s,
    f_r,
    c_s,
    c_r,
    h_s,
    h_r,
    bp_s,
    bp_r,
    st_s,
    st_r,
):
    rows, width = tok.shape
    ff = gw.shape[1]
    na, nbw, tiles = tiles_of(ff)
    nt = len(tiles)
    base_b = 2 * na
    part = rows // G
    half = part // 2
    piece = part // PIECES
    kh = width // 2
    full = float(width * G)

    b = lax.axis_index("cb")
    r = lax.axis_index("ra")
    p = lax.axis_index("dp")
    x = lax.rem(b, 2)
    y = b // 2
    to_x = {"cb": b + 1 - 2 * x}
    to_y = {"cb": b + 2 - 4 * y}
    to_d = {"cb": (G - 1) - b}
    twin = {"dp": 1 - p}
    sets = [r + 1 - 2 * lax.rem(r, 2), r + 2 - 4 * (r // 2), (G - 1) - r, r]
    to_z = [{"ra": s} for s in sets[:3]]

    barrier = pltpu.get_barrier_semaphore()
    greet = [to_x, to_y, to_d, twin] + to_z
    for peer in greet:
        pl.semaphore_signal(barrier, inc=1, device_id=peer, device_id_type=MESH)

    def at(start, size, align):
        return pl.ds(pl.multiple_of(start, align), size)

    def remote(src, dst, send, recv, peer):
        return pltpu.make_async_remote_copy(
            src_ref=src,
            dst_ref=dst,
            send_sem=send,
            recv_sem=recv,
            device_id=peer,
            device_id_type=MESH,
        )

    def a_cols(t, who):
        off, w = tiles[t][0]
        return at(who * na + off, w, LANE)

    def b_cols(t, who):
        off, w = tiles[t][1]
        return at(base_b + who * nbw + off, w, LANE)

    def load_send(kind, t):
        slot = t % 2
        src = (gw, uw)[kind % 2]
        cols = a_cols(t, 1 - x) if kind < 2 else b_cols(t, 1 - y)
        w = tiles[t][kind // 2][1]
        return pltpu.make_async_copy(
            src.at[at(p * kh, kh, kh), cols],
            stage.at[kind, pl.ds(slot * kh, kh), pl.ds(0, w)],
            stage_sem.at[kind, slot],
        )

    def load_own(kind, t):
        src = (gw, uw)[kind % 2]
        cols = a_cols(t, x) if kind < 2 else b_cols(t, y)
        w = tiles[t][kind // 2][1]
        return pltpu.make_async_copy(
            src.at[:, cols], stage.at[kind, :, pl.ds(0, w)], stage_sem.at[kind, 0]
        )

    def tile_rows(t):
        return pl.ds(pl.multiple_of(t * TILE, TILE), TILE)

    def load_d(t, slot):
        return pltpu.make_async_copy(dw.at[tile_rows(t), :], stage_d.at[slot], stage_d_sem.at[slot])

    for t in range(min(2, nt)):
        for kind in range(4):
            load_send(kind, t).start()
    for t in range(2):
        load_d(t, t).start()

    pl.semaphore_wait(barrier, len(greet))

    own_tok = []
    for i in range(PIECES):
        rows_i = at(r * part + i * piece, piece, piece)
        for j, peer in enumerate((to_x, to_y)):
            own_tok.append(
                remote(tok.at[rows_i, :], xt.at[j, rows_i, :], tok_s.at[j, i], tok_r.at[j, i], peer)
            )
    for copy in own_tok:
        copy.start()
    gains = []
    for j, peer in enumerate((to_x, to_y)):
        for i, ref in enumerate((ng, nb)):
            gains.append(remote(ref, gb.at[j, i], gb_s.at[j, i], gb_r.at[j, i], peer))
    for copy in gains:
        copy.start()

    wcopy = {}
    fcopy = {}
    for t in range(nt):
        for s in range(2):
            off, w = tiles[t][s]
            mine = (sa, sb)[s].at[:, :, pl.ds(off, w)]
            there = (wa, wb)[s].at[:, at(width + p * kh, kh, kh), pl.ds(off, w)]
            wcopy[t, s] = remote(mine, there, w_s.at[t, s], w_r.at[t, s], (to_x, to_y)[s])
            fcopy[t, s] = remote(there, there, f_s.at[t, s], f_r.at[t, s], twin)

    def send_weights(t):
        for kind in range(4):
            load_send(kind, t).wait()
            s, g = kind // 2, kind % 2
            off, w = tiles[t][s]
            (sa, sb)[s][g, :, off : off + w] = stage[kind, (t % 2) * kh : (t % 2 + 1) * kh, 0:w].astype(BF16)
            if t + 2 < nt:
                load_send(kind, t + 2).start()
        for s in range(2):
            wcopy[t, s].start()

    def put_stats(v, dst, col):
        total = jnp.sum(v, axis=1, keepdims=True)
        off = v - total * (1.0 / width)
        spread = jnp.sum(off * off, axis=1, keepdims=True)
        lane = lax.broadcasted_iota(jnp.int32, (v.shape[0], LANE), 1)
        both = jnp.where(lane == 0, total, spread)
        dst[0, :, pl.ds(col, v.shape[0])] = both.T[:8, :]

    def get_stats(src, col, n):
        parts = [src[i, 0:2, pl.ds(col, n)] for i in range(G)]
        mean = (parts[0][0:1] + parts[1][0:1] + parts[2][0:1] + parts[3][0:1]) / full
        spread = jnp.zeros_like(mean)
        for q in parts:
            d = q[0:1] * (1.0 / width) - mean
            spread = spread + q[1:2] + width * (d * d)
        inv = lax.rsqrt(spread / full + EPS)
        sub = lax.broadcasted_iota(jnp.int32, (LANE, n), 0)
        return jnp.where(sub == 0, mean, inv).T

    def swap_stats(buf, which):
        return [
            remote(buf.at[0], buf.at[1 + i], st_s.at[which, i], st_r.at[which, i], peer)
            for i, peer in enumerate((to_x, to_y, to_d))
        ]

    send_weights(0)
    for j in range(G):
        put_stats(tok[pl.ds(j * part, part), :].astype(F32), st, j * part)
    swap1 = swap_stats(st, 0)
    for copy in swap1:
        copy.start()

    def zcopy(way, dist, j, i):
        q = r - dist if way == 0 else r + dist
        rows_q = at(q * part + i * piece, piece, piece)
        ref = xt.at[j, rows_q, :]
        peer = {"ra": r + 1 if way == 0 else r - 1}
        return remote(ref, ref, z_s.at[way, dist, j, i], z_r.at[way, dist, j, i], peer)

    def spread_own(i):
        for j in range(2):
            own_tok[2 * i + j].wait_recv()
        for way in range(2):

            @pl.when((r < G - 1) if way == 0 else (r > 0))
            def _():
                for j in range(2):
                    zcopy(way, 0, j, i).start()

    def arrive(dist, i):
        for way in range(2):

            @pl.when((r >= dist) if way == 0 else (r <= G - 1 - dist))
            def _():
                q = r - dist if way == 0 else r + dist
                rows_q = at(q * part + i * piece, piece, piece)
                for j in range(2):
                    ref = xt.at[j, rows_q, :]
                    remote(
                        ref, ref, z_s.at[way, dist - 1, j, i], z_r.at[way, dist - 1, j, i], to_x
                    ).wait_recv()

            if dist < G - 1:

                @pl.when(
                    jnp.logical_and(r >= dist, r < G - 1)
                    if way == 0
                    else jnp.logical_and(r <= G - 1 - dist, r > 0)
                )
                def _():
                    for j in range(2):
                        zcopy(way, dist, j, i).start()

    for t in range(1, nt):
        send_weights(t)
    for kind in range(4):
        load_own(kind, 0).start()

    spread_own(0)
    spread_own(1)
    for t in range(nt):
        for kind in range(4):
            load_own(kind, t).wait()
            s, g = kind // 2, kind % 2
            off, w = tiles[t][s]
            (wa, wb)[s][g, 0:width, off : off + w] = stage[kind, :, 0:w].astype(BF16)
            if t + 1 < nt:
                load_own(kind, t + 1).start()
    spread_own(2)
    for copy in swap1:
        copy.wait_recv()
    for j in range(G):
        ms[pl.ds(j * part, part), :] = get_stats(st, j * part, part)
    spread_own(3)
    for copy in gains:
        copy.wait_recv()

    def cast_d(t, carry):
        slot = lax.rem(t, 2)
        load_d(t, slot).wait()
        wd[tile_rows(t), :] = stage_d[slot].astype(BF16)

        @pl.when(t + 2 < ff // TILE)
        def _():
            load_d(t + 2, slot).start()

        return carry

    lax.fori_loop(0, ff // TILE, cast_d, 0)

    def normalize(k):
        for i in range(2):
            rows_i = at(sets[k] * part + i * half, half, half)
            both = ms[rows_i, :]
            mean, inv = both[:, 0:1], both[:, 1:2]

            def norm(v, gain, bias):
                return ((v.astype(F32) - mean) * inv * gain + bias).astype(BF16)

            for lhs, j, side in ((la, 0, y), (lb, 1, x)):
                spot = at((i + side - 2 * i * side) * half, half, half)
                lhs[spot, 0:width] = norm(tok[rows_i, :], ng[...], nb[...])
                lhs[spot, width : 2 * width] = norm(xt[j, rows_i, :], gb[j, 0], gb[j, 1])

    ccopy = {}
    hcopy = {}
    for k in range(G):
        for t in range(nt):
            m = k * nt + t
            spot = pl.ds(k * half, half)
            for s in range(2):
                off, w = tiles[t][s]
                region = (ca, cb)[s].at[:, spot, pl.ds(off, w)]
                land = (ra, rb)[s].at[:, spot, pl.ds(off, w)]
                ccopy[m, s] = remote(region, land, c_s.at[s, m], c_r.at[s, m], (to_y, to_x)[s])
                side, who = ((y, x), (x, y))[s]
                cols = (a_cols, b_cols)[s]

                def block(side_, who_, lo, n):
                    return hid.at[at(sets[k] * part + side_ * half + lo, n, n), cols(t, who_)]

                own = block(side, who, 0, half)
                of_x = block(side, 1 - who, 0, half // 2) if s == 0 else block(1 - side, who, 0, half // 2)
                of_y = (
                    block(1 - side, who, half // 2, half // 2)
                    if s == 0
                    else block(side, 1 - who, half // 2, half // 2)
                )
                hcopy[m, s] = [
                    remote(own, own, h_s.at[s, 0, m], h_r.at[s, 0, m], to_x),
                    remote(own, own, h_s.at[s, 1, m], h_r.at[s, 1, m], to_y),
                    remote(of_x, of_x, h_s.at[s, 2, m], h_r.at[s, 2, m], to_y),
                    remote(of_y, of_y, h_s.at[s, 3, m], h_r.at[s, 3, m], to_x),
                ]

    def s1(m):
        k, t = m // nt, m % nt
        for s in range(2):
            off, w = tiles[t][s]
            lhs, wgt, keep, away = ((la, wa, pa, ca), (lb, wb, pb, cb))[s]

            def one(g, carry):
                acc = jnp.dot(lhs[...], wgt[g, :, off : off + w], preferred_element_type=F32)
                keep[g, k * half : (k + 1) * half, off : off + w] = acc[:half]
                away[g, k * half : (k + 1) * half, off : off + w] = acc[half:].astype(BF16)
                return carry

            lax.fori_loop(0, 2, one, 0)
            ccopy[m, s].start()

    def s2(m):
        k, t = m // nt, m % nt
        for s in range(2):
            ccopy[m, s].wait_recv()
            off, w = tiles[t][s]
            keep, got = ((pa, ra), (pb, rb))[s]
            side, who = ((y, x), (x, y))[s]
            cols = (a_cols, b_cols)[s](t, who)
            spot = pl.ds(k * half, half)
            g = keep[0, spot, off : off + w] + got[0, spot, off : off + w].astype(F32)
            u = keep[1, spot, off : off + w] + got[1, spot, off : off + w].astype(F32)
            g = g * gs[:, cols]
            u = u * us[:, cols]
            h = (g / (1.0 + jnp.exp(-g)) * u).astype(BF16)
            hid[at(sets[k] * part + side * half, half, half), cols] = h
            hcopy[m, s][0].start()
            hcopy[m, s][1].start()

    def s3(m):
        for s in range(2):
            hcopy[m, s][0].wait_recv()
            hcopy[m, s][2].start()
            hcopy[m, s][1].wait_recv()
            hcopy[m, s][3].start()

    zcp = [remote(bp.at[k], zr.at[k], bp_s.at[k], bp_r.at[k], to_z[k]) for k in range(G - 1)]

    def s4(k):
        for t in range(nt):
            for s in range(2):
                for i in (2, 3):
                    hcopy[k * nt + t, s][i].wait_recv()
        lhs = at(sets[k] * part, part, part)
        if k == G - 1:
            for copy in zcp:
                copy.wait_recv()

        def body(n, carry):
            cols = pl.ds(pl.multiple_of(n * TILE, TILE), TILE)
            acc = jnp.dot(hid[lhs, :], wd[:, cols], preferred_element_type=F32)
            if k < G - 1:
                bp[k, :, cols] = acc.astype(BF16)
            else:
                for q in range(G - 1):
                    acc = acc + zr[q, :, cols].astype(F32)
                acc = acc * down_scale[:, cols]
                for i in range(2):
                    spot = at((i + y - 2 * i * y) * half, half, half)
                    mix[i * half : (i + 1) * half, cols] = (
                        0.5 * la[spot, cols].astype(F32) + acc[i * half : (i + 1) * half]
                    )
            return carry

        lax.fori_loop(0, width // TILE, body, 0)
        if k < G - 1:
            zcp[k].start()

    def weights_in(t):
        for s in range(2):
            wcopy[t, s].wait_recv()
            fcopy[t, s].start()

    def weights_ready(t):
        for s in range(2):
            fcopy[t, s].wait_recv()

    for i in range(PIECES // 2):
        arrive(1, i)
    weights_in(0)
    for i in range(PIECES // 2, PIECES):
        arrive(1, i)
    normalize(0)
    weights_ready(0)

    steps = G * nt
    for i in range(steps + 4):
        if 0 < i < nt:
            weights_in(i)
            weights_ready(i)
        if i == nt:
            for j in range(PIECES):
                arrive(2, j)
        if i == 2 * nt:
            for j in range(PIECES):
                arrive(3, j)
        if i % nt == 0 and 0 < i < steps:
            normalize(i // nt)
        if i < steps:
            s1(i)
        if 0 <= i - 2 < steps:
            s2(i - 2)
        if 0 <= i - 3 < steps:
            s3(i - 3)
        if i - 4 >= 0 and (i - 4) % nt == nt - 1:
            s4((i - 4) // nt)

    put_stats(mix[...], st2, 0)
    swap2 = swap_stats(st2, 1)
    for copy in swap2:
        copy.start()
    for copy in swap2:
        copy.wait_recv()
    both = get_stats(st2, 0, part)
    out[...] = ((mix[...] - both[:, 0:1]) * both[:, 1:2] * og[...] + ob[...]).astype(BF16)

    for copy in swap1 + swap2 + own_tok + gains + zcp:
        copy.wait_send()
    for group in (wcopy, fcopy, ccopy):
        for copy in group.values():
            copy.wait_send()
    for group in hcopy.values():
        for copy in group:
            copy.wait_send()
    for way in range(2):
        for dist in range(G - 1):

            @pl.when(
                jnp.logical_and(r >= dist, r < G - 1)
                if way == 0
                else jnp.logical_and(r <= G - 1 - dist, r > 0)
            )
            def _():
                for i in range(PIECES):
                    for j in range(2):
                        zcopy(way, dist, j, i).wait_send()


def fused(
    tokens,
    norm_gain,
    norm_bias,
    gate_weight,
    up_weight,
    gate_scale,
    up_scale,
    down_weight,
    down_scale,
    out_gain,
    out_bias,
):
    rows, width = tokens.shape
    ff = gate_weight.shape[1]
    na, nbw, tiles = tiles_of(ff)
    nt = len(tiles)
    part = rows // G
    half = part // 2
    kh = width // 2
    steps = G * nt
    vmem = pl.BlockSpec(memory_space=pltpu.VMEM)
    hbm = pl.BlockSpec(memory_space=pl.ANY)
    row = lambda v: v.reshape(1, -1)
    dma = pltpu.SemaphoreType.DMA
    return pl.pallas_call(
        kernel,
        out_shape=jax.ShapeDtypeStruct((part, width), BF16),
        in_specs=[vmem, vmem, vmem, hbm, hbm, vmem, vmem, hbm, vmem, vmem, vmem],
        out_specs=vmem,
        scratch_shapes=[
            pltpu.VMEM((4, width, TILE), F32),
            pltpu.VMEM((2, TILE, width), F32),
            pltpu.VMEM((2, 2 * width, na), BF16),
            pltpu.VMEM((2, 2 * width, nbw), BF16),
            pltpu.VMEM((2, kh, na), BF16),
            pltpu.VMEM((2, kh, nbw), BF16),
            pltpu.VMEM((2, rows, width), BF16),
            pltpu.VMEM((2, 2, 1, width), F32),
            pltpu.VMEM((part, 2 * width), BF16),
            pltpu.VMEM((part, 2 * width), BF16),
            pltpu.VMEM((2, rows // 2, na), F32),
            pltpu.VMEM((2, rows // 2, nbw), F32),
            pltpu.VMEM((2, rows // 2, na), BF16),
            pltpu.VMEM((2, rows // 2, nbw), BF16),
            pltpu.VMEM((2, rows // 2, na), BF16),
            pltpu.VMEM((2, rows // 2, nbw), BF16),
            pltpu.VMEM((rows, ff), BF16),
            pltpu.VMEM((ff, width), BF16),
            pltpu.VMEM((G - 1, part, width), BF16),
            pltpu.VMEM((G - 1, part, width), BF16),
            pltpu.VMEM((part, width), F32),
            pltpu.VMEM((rows, LANE), F32),
            pltpu.VMEM((G, 8, rows), F32),
            pltpu.VMEM((G, 8, part), F32),
            dma((4, 2)),
            dma((2,)),
            dma((2, PIECES)),
            dma((2, PIECES)),
            dma((2, G - 1, 2, PIECES)),
            dma((2, G - 1, 2, PIECES)),
            dma((2, 2)),
            dma((2, 2)),
            dma((nt, 2)),
            dma((nt, 2)),
            dma((nt, 2)),
            dma((nt, 2)),
            dma((2, steps)),
            dma((2, steps)),
            dma((2, 4, steps)),
            dma((2, 4, steps)),
            dma((G - 1,)),
            dma((G - 1,)),
            dma((2, G - 1)),
            dma((2, G - 1)),
        ],
        compiler_params=pltpu.CompilerParams(
            collective_id=0, has_side_effects=True, vmem_limit_bytes=67043328
        ),
    )(
        tokens,
        row(norm_gain),
        row(norm_bias),
        gate_weight,
        up_weight,
        row(gate_scale),
        row(up_scale),
        down_weight,
        row(down_scale),
        row(out_gain),
        row(out_bias),
    )


def local(*args):
    rows, width = args[0].shape
    ff = args[3].shape[1]
    fits = (
        lax.axis_size("cb") == G
        and lax.axis_size("ra") == G
        and lax.axis_size("dp") == 2
        and rows % (256 * G) == 0
        and width % TILE == 0
        and ff % TILE == 0
        and min(pair[1][1] for pair in tiles_of(ff)[2]) > 0
        and rows * width <= 1 << 20
        and ff * width <= 2816 * 1024
    )
    return (fused if fits else plain)(*args)


def solution(mesh):
    return jax.shard_map(
        local,
        mesh=mesh,
        in_specs=(
            P("dp", "cb"),
            P("cb"),
            P("cb"),
            P("cb", "ra"),
            P("cb", "ra"),
            P("ra"),
            P("ra"),
            P("ra", "cb"),
            P("cb"),
            P("cb"),
            P("cb"),
        ),
        out_specs=P(("dp", "ra"), "cb"),
        check_vma=False,
    )
```

time: 184 us -> 166 us (0.902)
  the two profiles are of different devices: /device:TPU:0 before, /device:TPU:22 now
where the time goes in v1:
time: 166 us; the launch traced here: 165 us
  Pallas kernels  161 us (97%)
  local copies, waits for them, and re-layouts  4.49 us (3%)
    pallas_call x1, Pallas kernels, fused(): pl.pallas_call(kernel, out_shape=jax.ShapeDtypeStruct((part, width), BF16...  161 us

profile of v1, /device:TPU:22, one launch (start us, length us, event | category | flops | bytes accessed | tf_op | source)
XLA Modules:
  0.0 165.3 jit_solution(2353232059509711311)
XLA Ops:
  0.0 1.3 reshape.23.gs
  1.3 1.3 reshape.24.us
  2.6 160.8 %shard_map.109 = bf16[256,1024]{1,0:T(8,128)(2,1)} custom-call(bf16[1024,1024]{1,0:T(8,128)(2,1)} %tok.1, f32[1,1024]{1,0:T(1,128)} %bitcast.5, f32[1,1024]{1,0:T(1,128)} %bitcast.6, f32[1024,2816]{1,0:T(8,128)} %gw.1, f32[1024,2816]{1,0:T(8,128)} %uw.1, f32[1,2816]{1,0:T(1,128)} %reshape.23.gs, f32[1,2816]{1,0:T(1,128)} %reshape.24.us, f32[2816,1024]{1,0:T(8,128)} %dw.1, ...), custom_call_target="tpu_custom_call" | custom-call | tf_op jit(solution)/shard_map/pallas_call | solution.py:571
  163.4 1.9 %copy.13 = bf16[256,1024]{1,0:T(8,128)(2,1)} copy(bf16[256,1024]{1,0:T(8,128)(2,1)} %shard_map.109) | data formatting | bytes 1048576

commit v2 on v1

--- a/solution.py
+++ b/solution.py
@@ -10,6 +10,7 @@
 TILE = 256
 LANE = 128
 PIECES = 4
+SKEW = (1, 2, 3)
 G = 4
 F32 = jnp.float32
 BF16 = jnp.bfloat16
@@ -70,14 +71,23 @@
 
 
 def kernel(
+    tok_hbm,
+    ng_hbm,
+    nb_hbm,
+    gw,
+    uw,
+    gs_hbm,
+    us_hbm,
+    dw,
+    ds_hbm,
+    og_hbm,
+    ob_hbm,
+    out_hbm,
     tok,
     ng,
     nb,
-    gw,
-    uw,
     gs,
     us,
-    dw,
     down_scale,
     og,
     ob,
@@ -102,10 +112,13 @@
     wd,
     bp,
     zr,
+    zs,
     mix,
     ms,
     st,
     st2,
+    in_sem,
+    out_sem,
     stage_sem,
     stage_d_sem,
     tok_s,
@@ -124,6 +137,7 @@
     h_r,
     bp_s,
     bp_r,
+    zs_r,
     st_s,
     st_r,
 ):
@@ -147,13 +161,39 @@
     to_y = {"cb": b + 2 - 4 * y}
     to_d = {"cb": (G - 1) - b}
     twin = {"dp": 1 - p}
-    sets = [r + 1 - 2 * lax.rem(r, 2), r + 2 - 4 * (r // 2), (G - 1) - r, r]
+    hi = r // 2
+    sets = [3 - 3 * hi, 2 - hi, r + 1 - 2 * lax.rem(r, 2), r]
+    inner = lax.rem(r, 2) + hi == 1
     to_z = [{"ra": s} for s in sets[:3]]
+    ring = [{"ra": lax.rem(r + o, G)} for o in range(1, G)]
 
     barrier = pltpu.get_barrier_semaphore()
-    greet = [to_x, to_y, to_d, twin] + to_z
+    greet = [to_x, to_y, to_d, twin] + ring
     for peer in greet:
         pl.semaphore_signal(barrier, inc=1, device_id=peer, device_id_type=MESH)
+
+    small = [
+        pltpu.make_async_copy(src, dst, in_sem.at[G + i])
+        for i, (src, dst) in enumerate(
+            (
+                (ng_hbm, ng),
+                (nb_hbm, nb),
+                (gs_hbm, gs),
+                (us_hbm, us),
+                (ds_hbm, down_scale),
+                (og_hbm, og),
+                (ob_hbm, ob),
+            )
+        )
+    ]
+    tok_in = [
+        pltpu.make_async_copy(
+            tok_hbm.at[pl.ds(j * part, part), :], tok.at[pl.ds(j * part, part), :], in_sem.at[j]
+        )
+        for j in range(G)
+    ]
+    for copy in tok_in + small:
+        copy.start()
 
     def at(start, size, align):
         return pl.ds(pl.multiple_of(start, align), size)
@@ -207,14 +247,48 @@
     for t in range(2):
         load_d(t, t).start()
 
+    def put_stats(v, dst, col):
+        total = jnp.sum(v, axis=1, keepdims=True)
+        off = v - total * (1.0 / width)
+        spread = jnp.sum(off * off, axis=1, keepdims=True)
+        lane = lax.broadcasted_iota(jnp.int32, (v.shape[0], LANE), 1)
+        both = jnp.where(lane == 0, total, spread)
+        dst[0, :, pl.ds(col, v.shape[0])] = both.T[:8, :]
+
+    def get_stats(src, col, n):
+        parts = [src[i, 0:2, pl.ds(col, n)] for i in range(G)]
+        mean = (parts[0][0:1] + parts[1][0:1] + parts[2][0:1] + parts[3][0:1]) / full
+        spread = jnp.zeros_like(mean)
+        for q in parts:
+            d = q[0:1] * (1.0 / width) - mean
+            spread = spread + q[1:2] + width * (d * d)
+        inv = lax.rsqrt(spread / full + EPS)
+        sub = lax.broadcasted_iota(jnp.int32, (LANE, n), 0)
+        return jnp.where(sub == 0, mean, inv).T
+
+    def swap_stats(buf, which):
+        return [
+            remote(buf.at[0, pl.ds(0, 2)], buf.at[1 + i, pl.ds(0, 2)], st_s.at[which, i], st_r.at[which, i], peer)
+            for i, peer in enumerate((to_x, to_y, to_d))
+        ]
+
+    for j in range(G):
+        tok_in[j].wait()
+        put_stats(tok[pl.ds(j * part, part), :].astype(F32), st, j * part)
+    for copy in small:
+        copy.wait()
     pl.semaphore_wait(barrier, len(greet))
+
+    swap1 = swap_stats(st, 0)
+    for copy in swap1:
+        copy.start()
 
     own_tok = []
     for i in range(PIECES):
-        rows_i = at(r * part + i * piece, piece, piece)
+        rows_i = at((G - 1 - r) * part + i * piece, piece, piece)
         for j, peer in enumerate((to_x, to_y)):
             own_tok.append(
-                remote(tok.at[rows_i, :], xt.at[j, rows_i, :], tok_s.at[j, i], tok_r.at[j, i], peer)
+                remote(tok.at[rows_i, :], xt.at[j, rows_i, :], tok_s.at[j], tok_r.at[j, i], peer)
             )
     for copy in own_tok:
         copy.start()
@@ -232,8 +306,8 @@
             off, w = tiles[t][s]
             mine = (sa, sb)[s].at[:, :, pl.ds(off, w)]
             there = (wa, wb)[s].at[:, at(width + p * kh, kh, kh), pl.ds(off, w)]
-            wcopy[t, s] = remote(mine, there, w_s.at[t, s], w_r.at[t, s], (to_x, to_y)[s])
-            fcopy[t, s] = remote(there, there, f_s.at[t, s], f_r.at[t, s], twin)
+            wcopy[t, s] = remote(mine, there, w_s.at[s], w_r.at[t, s], (to_x, to_y)[s])
+            fcopy[t, s] = remote(there, there, f_s.at[s], f_r.at[t, s], twin)
 
     def send_weights(t):
         for kind in range(4):
@@ -246,44 +320,12 @@
         for s in range(2):
             wcopy[t, s].start()
 
-    def put_stats(v, dst, col):
-        total = jnp.sum(v, axis=1, keepdims=True)
-        off = v - total * (1.0 / width)
-        spread = jnp.sum(off * off, axis=1, keepdims=True)
-        lane = lax.broadcasted_iota(jnp.int32, (v.shape[0], LANE), 1)
-        both = jnp.where(lane == 0, total, spread)
-        dst[0, :, pl.ds(col, v.shape[0])] = both.T[:8, :]
-
-    def get_stats(src, col, n):
-        parts = [src[i, 0:2, pl.ds(col, n)] for i in range(G)]
-        mean = (parts[0][0:1] + parts[1][0:1] + parts[2][0:1] + parts[3][0:1]) / full
-        spread = jnp.zeros_like(mean)
-        for q in parts:
-            d = q[0:1] * (1.0 / width) - mean
-            spread = spread + q[1:2] + width * (d * d)
-        inv = lax.rsqrt(spread / full + EPS)
-        sub = lax.broadcasted_iota(jnp.int32, (LANE, n), 0)
-        return jnp.where(sub == 0, mean, inv).T
-
-    def swap_stats(buf, which):
-        return [
-            remote(buf.at[0], buf.at[1 + i], st_s.at[which, i], st_r.at[which, i], peer)
-            for i, peer in enumerate((to_x, to_y, to_d))
-        ]
-
-    send_weights(0)
-    for j in range(G):
-        put_stats(tok[pl.ds(j * part, part), :].astype(F32), st, j * part)
-    swap1 = swap_stats(st, 0)
-    for copy in swap1:
-        copy.start()
-
     def zcopy(way, dist, j, i):
         q = r - dist if way == 0 else r + dist
-        rows_q = at(q * part + i * piece, piece, piece)
+        rows_q = at((G - 1 - q) * part + i * piece, piece, piece)
         ref = xt.at[j, rows_q, :]
         peer = {"ra": r + 1 if way == 0 else r - 1}
-        return remote(ref, ref, z_s.at[way, dist, j, i], z_r.at[way, dist, j, i], peer)
+        return remote(ref, ref, z_s.at[way, dist], z_r.at[way, dist, j, i], peer)
 
     def spread_own(i):
         for j in range(2):
@@ -301,11 +343,11 @@
             @pl.when((r >= dist) if way == 0 else (r <= G - 1 - dist))
             def _():
                 q = r - dist if way == 0 else r + dist
-                rows_q = at(q * part + i * piece, piece, piece)
+                rows_q = at((G - 1 - q) * part + i * piece, piece, piece)
                 for j in range(2):
                     ref = xt.at[j, rows_q, :]
                     remote(
-                        ref, ref, z_s.at[way, dist - 1, j, i], z_r.at[way, dist - 1, j, i], to_x
+                        ref, ref, z_s.at[way, dist - 1], z_r.at[way, dist - 1, j, i], to_x
                     ).wait_recv()
 
             if dist < G - 1:
@@ -319,7 +361,7 @@
                     for j in range(2):
                         zcopy(way, dist, j, i).start()
 
-    for t in range(1, nt):
+    for t in range(nt):
         send_weights(t)
     for kind in range(4):
         load_own(kind, 0).start()
@@ -380,7 +422,7 @@
                 off, w = tiles[t][s]
                 region = (ca, cb)[s].at[:, spot, pl.ds(off, w)]
                 land = (ra, rb)[s].at[:, spot, pl.ds(off, w)]
-                ccopy[m, s] = remote(region, land, c_s.at[s, m], c_r.at[s, m], (to_y, to_x)[s])
+                ccopy[m, s] = remote(region, land, c_s.at[s], c_r.at[s, m], (to_y, to_x)[s])
                 side, who = ((y, x), (x, y))[s]
                 cols = (a_cols, b_cols)[s]
 
@@ -395,11 +437,16 @@
                     else block(side, 1 - who, half // 2, half // 2)
                 )
                 hcopy[m, s] = [
-                    remote(own, own, h_s.at[s, 0, m], h_r.at[s, 0, m], to_x),
-                    remote(own, own, h_s.at[s, 1, m], h_r.at[s, 1, m], to_y),
-                    remote(of_x, of_x, h_s.at[s, 2, m], h_r.at[s, 2, m], to_y),
-                    remote(of_y, of_y, h_s.at[s, 3, m], h_r.at[s, 3, m], to_x),
+                    remote(own, own, h_s.at[s, 0], h_r.at[s, 0, m], to_x),
+                    remote(own, own, h_s.at[s, 1], h_r.at[s, 1, m], to_y),
+                    remote(of_x, of_x, h_s.at[s, 2], h_r.at[s, 2, m], to_y),
+                    remote(of_y, of_y, h_s.at[s, 3], h_r.at[s, 3, m], to_x),
                 ]
+
+    def scale_row(ref, s, t, who):
+        off, w = tiles[t][s]
+        first = (s * base_b + who * (na, nbw)[s] + off) // LANE
+        return jnp.concatenate([ref[pl.ds(first + i, 1), :] for i in range(w // LANE)], axis=1)
 
     def s1(m):
         k, t = m // nt, m % nt
@@ -427,8 +474,8 @@
             spot = pl.ds(k * half, half)
             g = keep[0, spot, off : off + w] + got[0, spot, off : off + w].astype(F32)
             u = keep[1, spot, off : off + w] + got[1, spot, off : off + w].astype(F32)
-            g = g * gs[:, cols]
-            u = u * us[:, cols]
+            g = g * scale_row(gs, s, t, who)
+            u = u * scale_row(us, s, t, who)
             h = (g / (1.0 + jnp.exp(-g)) * u).astype(BF16)
             hid[at(sets[k] * part + side * half, half, half), cols] = h
             hcopy[m, s][0].start()
@@ -441,37 +488,89 @@
             hcopy[m, s][1].wait_recv()
             hcopy[m, s][3].start()
 
-    zcp = [remote(bp.at[k], zr.at[k], bp_s.at[k], bp_r.at[k], to_z[k]) for k in range(G - 1)]
-
-    def s4(k):
-        for t in range(nt):
-            for s in range(2):
-                for i in (2, 3):
-                    hcopy[k * nt + t, s][i].wait_recv()
+    def out_cols(n):
+        return pl.ds(pl.multiple_of(n * TILE, TILE), TILE)
+
+    def to_inner(k, n):
+        cols = out_cols(n)
+        return remote(bp.at[k, :, cols], zs.at[k, :, cols], bp_s.at[k], zs_r.at[k, n], to_z[2])
+
+    def to_owner(k, n):
+        cols = out_cols(n)
+        slot = k // 2
+        return remote(bp.at[k, :, cols], zr.at[slot, :, cols], bp_s.at[k], bp_r.at[slot, n], to_z[k])
+
+    def segments(t):
+        (off_a, wid_a), (off_b, wid_b) = tiles[t]
+        for who in range(2):
+            yield who * na + off_a, wid_a
+            yield base_b + who * nbw + off_b, wid_b
+
+    def relays_in(m):
+        for s in range(2):
+            for i in (2, 3):
+                hcopy[m, s][i].wait_recv()
+
+    nn = width // TILE
+
+    def s4(k, first, last):
+        if first == 0:
+            for t in range(nt):
+                relays_in(k * nt + t)
         lhs = at(sets[k] * part, part, part)
-        if k == G - 1:
-            for copy in zcp:
-                copy.wait_recv()
 
         def body(n, carry):
-            cols = pl.ds(pl.multiple_of(n * TILE, TILE), TILE)
-            acc = jnp.dot(hid[lhs, :], wd[:, cols], preferred_element_type=F32)
-            if k < G - 1:
-                bp[k, :, cols] = acc.astype(BF16)
+            cols = out_cols(n)
+            bp[k, :, cols] = jnp.dot(hid[lhs, :], wd[:, cols], preferred_element_type=F32).astype(BF16)
+            if k == G - 2:
+                to_owner(k, n).start()
             else:
-                for q in range(G - 1):
-                    acc = acc + zr[q, :, cols].astype(F32)
+
+                @pl.when(jnp.logical_not(inner))
+                def _():
+                    to_inner(k, n).start()
+
+            return carry
+
+        lax.fori_loop(first, last, body, 0)
+
+    def join(k):
+        @pl.when(inner)
+        def _():
+            def body(n, carry):
+                cols = out_cols(n)
+                to_inner(k, n).wait_recv()
+                bp[k, :, cols] = (bp[k, :, cols].astype(F32) + zs[k, :, cols].astype(F32)).astype(BF16)
+                to_owner(k, n).start()
+                return carry
+
+            lax.fori_loop(0, nn, body, 0)
+
+    def s5(t):
+        relays_in((G - 1) * nt + t)
+        lhs = at(sets[G - 1] * part, part, part)
+        late = t == nt - 1
+        for n in range(nn):
+            cols = pl.ds(n * TILE, TILE)
+            acc = sum(
+                jnp.dot(hid[lhs, lo : lo + w], wd[lo : lo + w, cols], preferred_element_type=F32)
+                for lo, w in segments(t)
+            )
+            if t > 0:
+                acc = acc + mix[:, cols]
+            if late:
+                for slot, k in ((0, 0), (1, 2)):
+                    to_owner(k, n).wait_recv()
+                    acc = acc + zr[slot, :, cols].astype(F32)
+            if late:
                 acc = acc * down_scale[:, cols]
                 for i in range(2):
                     spot = at((i + y - 2 * i * y) * half, half, half)
                     mix[i * half : (i + 1) * half, cols] = (
                         0.5 * la[spot, cols].astype(F32) + acc[i * half : (i + 1) * half]
                     )
-            return carry
-
-        lax.fori_loop(0, width // TILE, body, 0)
-        if k < G - 1:
-            zcp[k].start()
+            else:
+                mix[:, cols] = acc
 
     def weights_in(t):
         for s in range(2):
@@ -482,53 +581,60 @@
         for s in range(2):
             fcopy[t, s].wait_recv()
 
-    for i in range(PIECES // 2):
+    for i in range(PIECES - 1):
         arrive(1, i)
     weights_in(0)
-    for i in range(PIECES // 2, PIECES):
-        arrive(1, i)
-    normalize(0)
+    arrive(1, PIECES - 1)
     weights_ready(0)
 
     steps = G * nt
-    for i in range(steps + 4):
+    for i in range(steps + SKEW[2]):
         if 0 < i < nt:
             weights_in(i)
             weights_ready(i)
-        if i == nt:
-            for j in range(PIECES):
-                arrive(2, j)
-        if i == 2 * nt:
-            for j in range(PIECES):
-                arrive(3, j)
-        if i % nt == 0 and 0 < i < steps:
+        if i % nt == 0 and i < steps:
+            if i // nt == G - 1:
+                for j in range(PIECES):
+                    arrive(G - 1, j)
             normalize(i // nt)
         if i < steps:
             s1(i)
-        if 0 <= i - 2 < steps:
-            s2(i - 2)
-        if 0 <= i - 3 < steps:
-            s3(i - 3)
-        if i - 4 >= 0 and (i - 4) % nt == nt - 1:
-            s4((i - 4) // nt)
+        if 0 <= i - nt < PIECES // 2:
+            arrive(2, 2 * (i - nt))
+            arrive(2, 2 * (i - nt) + 1)
+        if 0 <= i - SKEW[0] < steps:
+            s2(i - SKEW[0])
+        if 0 <= i - SKEW[1] < steps:
+            s3(i - SKEW[1])
+        m = i - SKEW[2]
+        if m >= 0 and m % nt == nt - 1 and 0 < m // nt < G - 1:
+            join(m // nt - 1)
+        if 0 <= m < steps - nt and m % nt == nt - 1:
+            s4(m // nt, 0, nn // 2 if m // nt < G - 2 else nn)
+        if nt <= m < steps - nt and m % nt == 0:
+            s4(m // nt - 1, nn // 2, nn)
+        if steps - nt <= m < steps:
+            s5(m - (steps - nt))
 
     put_stats(mix[...], st2, 0)
     swap2 = swap_stats(st2, 1)
     for copy in swap2:
         copy.start()
-    for copy in swap2:
-        copy.wait_recv()
-    both = get_stats(st2, 0, part)
-    out[...] = ((mix[...] - both[:, 0:1]) * both[:, 1:2] * og[...] + ob[...]).astype(BF16)
-
-    for copy in swap1 + swap2 + own_tok + gains + zcp:
+    for copy in swap1 + gains:
         copy.wait_send()
-    for group in (wcopy, fcopy, ccopy):
-        for copy in group.values():
-            copy.wait_send()
-    for group in hcopy.values():
-        for copy in group:
-            copy.wait_send()
+    for k in range(G - 1):
+        remote(bp.at[k], bp.at[k], bp_s.at[k], bp_r.at[0, 0], to_x).wait_send()
+    for j in range(2):
+        ref = tok.at[pl.ds(0, part), :]
+        remote(ref, ref, tok_s.at[j], tok_r.at[j, 0], to_x).wait_send()
+    for s in range(2):
+        mine, away = ((sa, ca), (sb, cb))[s]
+        remote(mine, mine, w_s.at[s], w_r.at[0, s], to_x).wait_send()
+        remote(mine, mine, f_s.at[s], f_r.at[0, s], to_x).wait_send()
+        remote(away, away, c_s.at[s], c_r.at[s, 0], to_x).wait_send()
+        for i in range(4):
+            ref = away.at[0] if i < 2 else away.at[0, pl.ds(0, rows // 4)]
+            remote(ref, ref, h_s.at[s, i], h_r.at[s, i, 0], to_x).wait_send()
     for way in range(2):
         for dist in range(G - 1):
 
@@ -538,9 +644,23 @@
                 else jnp.logical_and(r <= G - 1 - dist, r > 0)
             )
             def _():
-                for i in range(PIECES):
-                    for j in range(2):
-                        zcopy(way, dist, j, i).wait_send()
+                ref = xt.at[:, pl.ds(0, part), :]
+                remote(ref, ref, z_s.at[way, dist], z_r.at[way, dist, 0, 0], to_x).wait_send()
+    for copy in swap2:
+        copy.wait_recv()
+    both = get_stats(st2, 0, part)
+    final = []
+    for i in range(2):
+        spot = pl.ds(i * half, half)
+        mean, inv = both[i * half : (i + 1) * half, 0:1], both[i * half : (i + 1) * half, 1:2]
+        out[spot, :] = ((mix[spot, :] - mean) * inv * og[...] + ob[...]).astype(BF16)
+        final.append(pltpu.make_async_copy(out.at[spot, :], out_hbm.at[spot, :], out_sem.at[i]))
+        final[i].start()
+
+    for copy in swap2:
+        copy.wait_send()
+    for copy in final:
+        copy.wait()
 
 
 def fused(
@@ -564,16 +684,24 @@
     half = part // 2
     kh = width // 2
     steps = G * nt
-    vmem = pl.BlockSpec(memory_space=pltpu.VMEM)
     hbm = pl.BlockSpec(memory_space=pl.ANY)
     row = lambda v: v.reshape(1, -1)
     dma = pltpu.SemaphoreType.DMA
     return pl.pallas_call(
         kernel,
         out_shape=jax.ShapeDtypeStruct((part, width), BF16),
-        in_specs=[vmem, vmem, vmem, hbm, hbm, vmem, vmem, hbm, vmem, vmem, vmem],
-        out_specs=vmem,
+        in_specs=[hbm] * 11,
+        out_specs=hbm,
         scratch_shapes=[
+            pltpu.VMEM((rows, width), BF16),
+            pltpu.VMEM((1, width), F32),
+            pltpu.VMEM((1, width), F32),
+            pltpu.VMEM((ff // LANE, LANE), F32),
+            pltpu.VMEM((ff // LANE, LANE), F32),
+            pltpu.VMEM((1, width), F32),
+            pltpu.VMEM((1, width), F32),
+            pltpu.VMEM((1, width), F32),
+            pltpu.VMEM((part, width), BF16),
             pltpu.VMEM((4, width, TILE), F32),
             pltpu.VMEM((2, TILE, width), F32),
             pltpu.VMEM((2, 2 * width, na), BF16),
@@ -593,29 +721,33 @@
             pltpu.VMEM((rows, ff), BF16),
             pltpu.VMEM((ff, width), BF16),
             pltpu.VMEM((G - 1, part, width), BF16),
-            pltpu.VMEM((G - 1, part, width), BF16),
+            pltpu.VMEM((2, part, width), BF16),
+            pltpu.VMEM((2, part, width), BF16),
             pltpu.VMEM((part, width), F32),
             pltpu.VMEM((rows, LANE), F32),
             pltpu.VMEM((G, 8, rows), F32),
             pltpu.VMEM((G, 8, part), F32),
+            dma((G + 7,)),
+            dma((2,)),
             dma((4, 2)),
             dma((2,)),
+            dma((2,)),
             dma((2, PIECES)),
-            dma((2, PIECES)),
-            dma((2, G - 1, 2, PIECES)),
+            dma((2, G - 1)),
             dma((2, G - 1, 2, PIECES)),
             dma((2, 2)),
             dma((2, 2)),
+            dma((2,)),
             dma((nt, 2)),
+            dma((2,)),
             dma((nt, 2)),
-            dma((nt, 2)),
-            dma((nt, 2)),
+            dma((2,)),
             dma((2, steps)),
-            dma((2, steps)),
-            dma((2, 4, steps)),
+            dma((2, 4)),
             dma((2, 4, steps)),
             dma((G - 1,)),
-            dma((G - 1,)),
+            dma((2, width // TILE)),
+            dma((2, width // TILE)),
             dma((2, G - 1)),
             dma((2, G - 1)),
         ],
@@ -628,8 +760,8 @@
         row(norm_bias),
         gate_weight,
         up_weight,
-        row(gate_scale),
-        row(up_scale),
+        gate_scale.reshape(-1, LANE),
+        up_scale.reshape(-1, LANE),
         down_weight,
         row(down_scale),
         row(out_gain),

time: 166 us -> 142 us (0.86)
  the two profiles are of different devices: /device:TPU:22 before, /device:TPU:0 now
where the time goes in v2:
time: 142 us; the launch traced here: 141 us
  Pallas kernels  139 us (98%)
  local copies, waits for them, and re-layouts  1.87 us (1%)
    pallas_call x1, Pallas kernels, fused(): pl.pallas_call(kernel, out_shape=jax.ShapeDtypeStruct((part, width), BF16...  139 us

profile of v2, /device:TPU:0, one launch (start us, length us, event | category | flops | bytes accessed | tf_op | source)
XLA Modules:
  0.0 141.0 jit_solution(4109960091876106293)
XLA Ops:
  0.0 139.1 %shard_map.109 = bf16[256,1024]{1,0:T(8,128)(2,1)} custom-call(bf16[1024,1024]{1,0:T(8,128)(2,1)} %tok_hbm.1, f32[1,1024]{1,0:T(1,128)} %bitcast.9, f32[1,1024]{1,0:T(1,128)} %bitcast.10, f32[1024,2816]{1,0:T(8,128)} %gw.1, f32[1024,2816]{1,0:T(8,128)} %uw.1, f32[22,128]{1,0:T(8,128)} %bitcast.7, f32[22,128]{1,0:T(8,128)} %bitcast.8, f32[2816,1024]{1,0:T(8,128)} %dw.1, ...), custom_call_target="tpu_custom_call" | custom-call | tf_op jit(solution)/shard_map/pallas_call | solution.py:690
  139.1 1.9 %copy.13 = bf16[256,1024]{1,0:T(8,128)(2,1)} copy(bf16[256,1024]{1,0:T(8,128)(2,1)} %shard_map.109) | data formatting | bytes 1048576

commit v3 on v2

--- a/solution.py
+++ b/solution.py
@@ -10,7 +10,6 @@
 TILE = 256
 LANE = 128
 PIECES = 4
-SKEW = (1, 2, 3)
 G = 4
 F32 = jnp.float32
 BF16 = jnp.bfloat16
@@ -82,7 +81,7 @@
     ds_hbm,
     og_hbm,
     ob_hbm,
-    out_hbm,
+    out,
     tok,
     ng,
     nb,
@@ -91,7 +90,6 @@
     down_scale,
     og,
     ob,
-    out,
     stage,
     stage_d,
     wa,
@@ -118,7 +116,6 @@
     st,
     st2,
     in_sem,
-    out_sem,
     stage_sem,
     stage_d_sem,
     tok_s,
@@ -188,9 +185,11 @@
     ]
     tok_in = [
         pltpu.make_async_copy(
-            tok_hbm.at[pl.ds(j * part, part), :], tok.at[pl.ds(j * part, part), :], in_sem.at[j]
+            tok_hbm.at[pl.ds(pl.multiple_of(q * part, part), part), :],
+            tok.at[pl.ds(pl.multiple_of(q * part, part), part), :],
+            in_sem.at[j],
         )
-        for j in range(G)
+        for j, q in enumerate(lax.rem(G - 1 - r + j, G) for j in range(G))
     ]
     for copy in tok_in + small:
         copy.start()
@@ -247,6 +246,21 @@
     for t in range(2):
         load_d(t, t).start()
 
+    tok_in[0].wait()
+    pl.semaphore_wait(barrier, len(greet))
+
+    own_tok = []
+    for i in range(PIECES):
+        rows_i = at((G - 1 - r) * part + i * piece, piece, piece)
+        for j, peer in enumerate((to_x, to_y)):
+            own_tok.append(
+                remote(tok.at[rows_i, :], xt.at[j, rows_i, :], tok_s.at[j], tok_r.at[j, i], peer)
+            )
+    for copy in own_tok:
+        copy.start()
+    for copy in tok_in[1:] + small:
+        copy.wait()
+
     def put_stats(v, dst, col):
         total = jnp.sum(v, axis=1, keepdims=True)
         off = v - total * (1.0 / width)
@@ -273,24 +287,9 @@
         ]
 
     for j in range(G):
-        tok_in[j].wait()
         put_stats(tok[pl.ds(j * part, part), :].astype(F32), st, j * part)
-    for copy in small:
-        copy.wait()
-    pl.semaphore_wait(barrier, len(greet))
-
     swap1 = swap_stats(st, 0)
     for copy in swap1:
-        copy.start()
-
-    own_tok = []
-    for i in range(PIECES):
-        rows_i = at((G - 1 - r) * part + i * piece, piece, piece)
-        for j, peer in enumerate((to_x, to_y)):
-            own_tok.append(
-                remote(tok.at[rows_i, :], xt.at[j, rows_i, :], tok_s.at[j], tok_r.at[j, i], peer)
-            )
-    for copy in own_tok:
         copy.start()
     gains = []
     for j, peer in enumerate((to_x, to_y)):
@@ -399,6 +398,7 @@
     lax.fori_loop(0, ff // TILE, cast_d, 0)
 
     def normalize(k):
+        slot = k % 2
         for i in range(2):
             rows_i = at(sets[k] * part + i * half, half, half)
             both = ms[rows_i, :]
@@ -409,8 +409,8 @@
 
             for lhs, j, side in ((la, 0, y), (lb, 1, x)):
                 spot = at((i + side - 2 * i * side) * half, half, half)
-                lhs[spot, 0:width] = norm(tok[rows_i, :], ng[...], nb[...])
-                lhs[spot, width : 2 * width] = norm(xt[j, rows_i, :], gb[j, 0], gb[j, 1])
+                lhs[slot, spot, 0:width] = norm(tok[rows_i, :], ng[...], nb[...])
+                lhs[slot, spot, width : 2 * width] = norm(xt[j, rows_i, :], gb[j, 0], gb[j, 1])
 
     ccopy = {}
     hcopy = {}
@@ -455,7 +455,7 @@
             lhs, wgt, keep, away = ((la, wa, pa, ca), (lb, wb, pb, cb))[s]
 
             def one(g, carry):
-                acc = jnp.dot(lhs[...], wgt[g, :, off : off + w], preferred_element_type=F32)
+                acc = jnp.dot(lhs[k % 2], wgt[g, :, off : off + w], preferred_element_type=F32)
                 keep[g, k * half : (k + 1) * half, off : off + w] = acc[:half]
                 away[g, k * half : (k + 1) * half, off : off + w] = acc[half:].astype(BF16)
                 return carry
@@ -463,9 +463,9 @@
             lax.fori_loop(0, 2, one, 0)
             ccopy[m, s].start()
 
-    def s2(m):
+    def s2(m, sides=(0, 1)):
         k, t = m // nt, m % nt
-        for s in range(2):
+        for s in sides:
             ccopy[m, s].wait_recv()
             off, w = tiles[t][s]
             keep, got = ((pa, ra), (pb, rb))[s]
@@ -567,7 +567,7 @@
                 for i in range(2):
                     spot = at((i + y - 2 * i * y) * half, half, half)
                     mix[i * half : (i + 1) * half, cols] = (
-                        0.5 * la[spot, cols].astype(F32) + acc[i * half : (i + 1) * half]
+                        0.5 * la[(G - 1) % 2, spot, cols].astype(F32) + acc[i * half : (i + 1) * half]
                     )
             else:
                 mix[:, cols] = acc
@@ -581,40 +581,64 @@
         for s in range(2):
             fcopy[t, s].wait_recv()
 
+    steps = G * nt
+    first = 2 * nt
+
     for i in range(PIECES - 1):
         arrive(1, i)
     weights_in(0)
     arrive(1, PIECES - 1)
+    normalize(0)
+    normalize(1)
     weights_ready(0)
-
-    steps = G * nt
-    for i in range(steps + SKEW[2]):
-        if 0 < i < nt:
-            weights_in(i)
-            weights_ready(i)
-        if i % nt == 0 and i < steps:
-            if i // nt == G - 1:
+    s1(0)
+    s1(nt)
+    for t in range(1, nt):
+        if t == nt - 1:
+            s2(0, (0,))
+        weights_in(t)
+        weights_ready(t)
+        s1(t)
+        if t == nt - 1:
+            s2(0, (1,))
+        s1(nt + t)
+        for j in range(PIECES):
+            if 1 + j * (nt - 1) // PIECES == t:
+                arrive(2, j)
+    for i in range(2, first):
+        if i == first - 1:
+            normalize(2)
+            s1(first)
+        s2(i - 1)
+        s3(i - 2)
+    s4(0, 0, nn)
+
+    for i in range(first, steps + 3):
+        if i < steps and i > first:
+            if i == steps - nt:
                 for j in range(PIECES):
                     arrive(G - 1, j)
-            normalize(i // nt)
-        if i < steps:
+                normalize(G - 1)
             s1(i)
-        if 0 <= i - nt < PIECES // 2:
-            arrive(2, 2 * (i - nt))
-            arrive(2, 2 * (i - nt) + 1)
-        if 0 <= i - SKEW[0] < steps:
-            s2(i - SKEW[0])
-        if 0 <= i - SKEW[1] < steps:
-            s3(i - SKEW[1])
-        m = i - SKEW[2]
-        if m >= 0 and m % nt == nt - 1 and 0 < m // nt < G - 1:
-            join(m // nt - 1)
-        if 0 <= m < steps - nt and m % nt == nt - 1:
-            s4(m // nt, 0, nn // 2 if m // nt < G - 2 else nn)
-        if nt <= m < steps - nt and m % nt == 0:
-            s4(m // nt - 1, nn // 2, nn)
-        if steps - nt <= m < steps:
-            s5(m - (steps - nt))
+        k = i // nt - 1
+        edge = i % nt == nt - 1 and k < G - 1
+        early = i == steps - nt + 1
+        if early:
+            s3(i - 2)
+        if i - 1 < steps:
+            s2(i - 1)
+        if edge and k == 2:
+            join(1)
+            s4(2, 0, nn)
+        if not early and i - 2 < steps:
+            s3(i - 2)
+        if edge:
+            if k < 2:
+                s4(k, 0, nn)
+            if k == 1:
+                join(0)
+        if i >= steps and i - steps < nt:
+            s5(i - steps)
 
     put_stats(mix[...], st2, 0)
     swap2 = swap_stats(st2, 1)
@@ -649,18 +673,13 @@
     for copy in swap2:
         copy.wait_recv()
     both = get_stats(st2, 0, part)
-    final = []
     for i in range(2):
         spot = pl.ds(i * half, half)
         mean, inv = both[i * half : (i + 1) * half, 0:1], both[i * half : (i + 1) * half, 1:2]
         out[spot, :] = ((mix[spot, :] - mean) * inv * og[...] + ob[...]).astype(BF16)
-        final.append(pltpu.make_async_copy(out.at[spot, :], out_hbm.at[spot, :], out_sem.at[i]))
-        final[i].start()
 
     for copy in swap2:
         copy.wait_send()
-    for copy in final:
-        copy.wait()
 
 
 def fused(
@@ -689,9 +708,9 @@
     dma = pltpu.SemaphoreType.DMA
     return pl.pallas_call(
         kernel,
-        out_shape=jax.ShapeDtypeStruct((part, width), BF16),
+        out_shape=pltpu.VMEM((part, width), BF16),
         in_specs=[hbm] * 11,
-        out_specs=hbm,
+        out_specs=pl.BlockSpec(memory_space=pltpu.VMEM),
         scratch_shapes=[
             pltpu.VMEM((rows, width), BF16),
             pltpu.VMEM((1, width), F32),
@@ -701,7 +720,6 @@
             pltpu.VMEM((1, width), F32),
             pltpu.VMEM((1, width), F32),
             pltpu.VMEM((1, width), F32),
-            pltpu.VMEM((part, width), BF16),
             pltpu.VMEM((4, width, TILE), F32),
             pltpu.VMEM((2, TILE, width), F32),
             pltpu.VMEM((2, 2 * width, na), BF16),
@@ -710,8 +728,8 @@
             pltpu.VMEM((2, kh, nbw), BF16),
             pltpu.VMEM((2, rows, width), BF16),
             pltpu.VMEM((2, 2, 1, width), F32),
-            pltpu.VMEM((part, 2 * width), BF16),
-            pltpu.VMEM((part, 2 * width), BF16),
+            pltpu.VMEM((2, part, 2 * width), BF16),
+            pltpu.VMEM((2, part, 2 * width), BF16),
             pltpu.VMEM((2, rows // 2, na), F32),
             pltpu.VMEM((2, rows // 2, nbw), F32),
             pltpu.VMEM((2, rows // 2, na), BF16),
@@ -728,7 +746,6 @@
             pltpu.VMEM((G, 8, rows), F32),
             pltpu.VMEM((G, 8, part), F32),
             dma((G + 7,)),
-            dma((2,)),
             dma((4, 2)),
             dma((2,)),
             dma((2,)),
@@ -752,7 +769,7 @@
             dma((2, G - 1)),
         ],
         compiler_params=pltpu.CompilerParams(
-            collective_id=0, has_side_effects=True, vmem_limit_bytes=67043328
+            collective_id=0, has_side_effects=True, vmem_limit_bytes=63500000
         ),
     )(
         tokens,

time: 142 us -> 138 us (0.972)
  Pallas kernels: 139 us -> 137 us
    pallas_call x1, Pallas kernels: 139 us -> 137 us  [fused(): pl.pallas_call(kernel, out_shape=pltpu.VMEM((part, width), BF16), in_spec...]
where the time goes in v3:
time: 138 us
  Pallas kernels  137 us (99%)
    pallas_call x1, Pallas kernels, fused(): pl.pallas_call(kernel, out_shape=pltpu.VMEM((part, width), BF16), in_spec...  137 us

profile of v3, /device:TPU:0, one launch (start us, length us, event | category | flops | bytes accessed | tf_op | source)
XLA Modules:
  0.0 138.1 jit_solution(11107471826123034663)
XLA Ops:
  0.0 137.3 %shard_map.109 = bf16[256,1024]{1,0:T(8,128)(2,1)S(1)} custom-call(bf16[1024,1024]{1,0:T(8,128)(2,1)} %tok_hbm.1, f32[1,1024]{1,0:T(1,128)} %bitcast.9, f32[1,1024]{1,0:T(1,128)} %bitcast.10, f32[1024,2816]{1,0:T(8,128)} %gw.1, f32[1024,2816]{1,0:T(8,128)} %uw.1, f32[22,128]{1,0:T(8,128)} %bitcast.7, f32[22,128]{1,0:T(8,128)} %bitcast.8, f32[2816,1024]{1,0:T(8,128)} %dw.1, ...), custom_call_target="tpu_custom_call" | custom-call | tf_op jit(solution)/shard_map/pallas_call | solution.py:709
  137.3 0.8 copy.13

commit v4 on v3

--- a/solution.py
+++ b/solution.py
@@ -324,7 +324,7 @@
         rows_q = at((G - 1 - q) * part + i * piece, piece, piece)
         ref = xt.at[j, rows_q, :]
         peer = {"ra": r + 1 if way == 0 else r - 1}
-        return remote(ref, ref, z_s.at[way, dist], z_r.at[way, dist, j, i], peer)
+        return remote(ref, ref, z_s.at[way, dist], z_r.at[way, dist, i], peer)
 
     def spread_own(i):
         for j in range(2):
@@ -343,11 +343,8 @@
             def _():
                 q = r - dist if way == 0 else r + dist
                 rows_q = at((G - 1 - q) * part + i * piece, piece, piece)
-                for j in range(2):
-                    ref = xt.at[j, rows_q, :]
-                    remote(
-                        ref, ref, z_s.at[way, dist - 1], z_r.at[way, dist - 1, j, i], to_x
-                    ).wait_recv()
+                ref = xt.at[:, rows_q, :]
+                remote(ref, ref, z_s.at[way, dist - 1], z_r.at[way, dist - 1, i], to_x).wait_recv()
 
             if dist < G - 1:
 
@@ -437,10 +434,10 @@
                     else block(side, 1 - who, half // 2, half // 2)
                 )
                 hcopy[m, s] = [
-                    remote(own, own, h_s.at[s, 0], h_r.at[s, 0, m], to_x),
-                    remote(own, own, h_s.at[s, 1], h_r.at[s, 1, m], to_y),
-                    remote(of_x, of_x, h_s.at[s, 2], h_r.at[s, 2, m], to_y),
-                    remote(of_y, of_y, h_s.at[s, 3], h_r.at[s, 3, m], to_x),
+                    remote(own, own, h_s.at[s, 0], h_r.at[2 * s, m], to_x),
+                    remote(own, own, h_s.at[s, 1], h_r.at[2 * s + 1, m], to_y),
+                    remote(of_x, of_x, h_s.at[s, 2], h_r.at[4, m], to_y),
+                    remote(of_y, of_y, h_s.at[s, 3], h_r.at[4, m], to_x),
                 ]
 
     def scale_row(ref, s, t, who):
@@ -507,9 +504,9 @@
             yield base_b + who * nbw + off_b, wid_b
 
     def relays_in(m):
-        for s in range(2):
-            for i in (2, 3):
-                hcopy[m, s][i].wait_recv()
+        (_, wid_a), (_, wid_b) = tiles[m % nt]
+        ref = hid.at[pl.ds(0, half), pl.ds(0, wid_a + wid_b)]
+        remote(ref, ref, h_s.at[0, 2], h_r.at[4, m], to_x).wait_recv()
 
     nn = width // TILE
 
@@ -533,6 +530,34 @@
             return carry
 
         lax.fori_loop(first, last, body, 0)
+
+    def partial(lhs, cols, steps_in):
+        return sum(
+            jnp.dot(hid[lhs, lo : lo + w], wd[lo : lo + w, cols], preferred_element_type=F32)
+            for t in steps_in
+            for lo, w in segments(t)
+        )
+
+    def s4_head(k):
+        for t in range(nt - 1):
+            relays_in(k * nt + t)
+        lhs = at(sets[k] * part, part, part)
+
+        def body(n, carry):
+            cols = out_cols(n)
+            mix[:, cols] = partial(lhs, cols, range(nt - 1))
+            return carry
+
+        lax.fori_loop(0, nn, body, 0)
+
+    def s4_tail(k):
+        relays_in(k * nt + nt - 1)
+        lhs = at(sets[k] * part, part, part)
+        for n in range(nn):
+            cols = out_cols(n)
+            acc = mix[:, cols] + partial(lhs, cols, (nt - 1,))
+            bp[k, :, cols] = acc.astype(BF16)
+            to_owner(k, n).start()
 
     def join(k):
         @pl.when(inner)
@@ -552,10 +577,7 @@
         late = t == nt - 1
         for n in range(nn):
             cols = pl.ds(n * TILE, TILE)
-            acc = sum(
-                jnp.dot(hid[lhs, lo : lo + w], wd[lo : lo + w, cols], preferred_element_type=F32)
-                for lo, w in segments(t)
-            )
+            acc = partial(lhs, cols, (t,))
             if t > 0:
                 acc = acc + mix[:, cols]
             if late:
@@ -614,8 +636,11 @@
     s4(0, 0, nn)
 
     for i in range(first, steps + 3):
+        border = i == steps - nt
+        if border:
+            s2(i - 1)
         if i < steps and i > first:
-            if i == steps - nt:
+            if border:
                 for j in range(PIECES):
                     arrive(G - 1, j)
                 normalize(G - 1)
@@ -625,11 +650,13 @@
         early = i == steps - nt + 1
         if early:
             s3(i - 2)
-        if i - 1 < steps:
+        if edge and k == 2:
+            s4_head(2)
+        if not border and i - 1 < steps:
             s2(i - 1)
         if edge and k == 2:
             join(1)
-            s4(2, 0, nn)
+            s4_tail(2)
         if not early and i - 2 < steps:
             s3(i - 2)
         if edge:
@@ -658,7 +685,7 @@
         remote(away, away, c_s.at[s], c_r.at[s, 0], to_x).wait_send()
         for i in range(4):
             ref = away.at[0] if i < 2 else away.at[0, pl.ds(0, rows // 4)]
-            remote(ref, ref, h_s.at[s, i], h_r.at[s, i, 0], to_x).wait_send()
+            remote(ref, ref, h_s.at[s, i], h_r.at[4, 0], to_x).wait_send()
     for way in range(2):
         for dist in range(G - 1):
 
@@ -669,7 +696,7 @@
             )
             def _():
                 ref = xt.at[:, pl.ds(0, part), :]
-                remote(ref, ref, z_s.at[way, dist], z_r.at[way, dist, 0, 0], to_x).wait_send()
+                remote(ref, ref, z_s.at[way, dist], z_r.at[way, dist, 0], to_x).wait_send()
     for copy in swap2:
         copy.wait_recv()
     both = get_stats(st2, 0, part)
@@ -751,7 +778,7 @@
             dma((2,)),
             dma((2, PIECES)),
             dma((2, G - 1)),
-            dma((2, G - 1, 2, PIECES)),
+            dma((2, G - 1, PIECES)),
             dma((2, 2)),
             dma((2, 2)),
             dma((2,)),
@@ -761,7 +788,7 @@
             dma((2,)),
             dma((2, steps)),
             dma((2, 4)),
-            dma((2, 4, steps)),
+            dma((5, steps)),
             dma((G - 1,)),
             dma((2, width // TILE)),
             dma((2, width // TILE)),

time: 138 us -> 138 us (level)
  no operation moved by 1% of the time
where the time goes in v4:
time: 138 us; the launch traced here: 137 us
  Pallas kernels  137 us (99%)
    pallas_call x1, Pallas kernels, fused(): pl.pallas_call(kernel, out_shape=pltpu.VMEM((part, width), BF16), in_spec...  137 us

profile of v4, /device:TPU:0, one launch (start us, length us, event | category | flops | bytes accessed | tf_op | source)
XLA Modules:
  0.0 137.3 jit_solution(4936807518167111653)
XLA Ops:
  0.0 136.5 %shard_map.109 = bf16[256,1024]{1,0:T(8,128)(2,1)S(1)} custom-call(bf16[1024,1024]{1,0:T(8,128)(2,1)} %tok_hbm.1, f32[1,1024]{1,0:T(1,128)} %bitcast.9, f32[1,1024]{1,0:T(1,128)} %bitcast.10, f32[1024,2816]{1,0:T(8,128)} %gw.1, f32[1024,2816]{1,0:T(8,128)} %uw.1, f32[22,128]{1,0:T(8,128)} %bitcast.7, f32[22,128]{1,0:T(8,128)} %bitcast.8, f32[2816,1024]{1,0:T(8,128)} %dw.1, ...), custom_call_target="tpu_custom_call" | custom-call | tf_op jit(solution)/shard_map/pallas_call | solution.py:736
  136.5 0.8 copy.13

commit v5 on v4

--- a/solution.py
+++ b/solution.py
@@ -294,7 +294,7 @@
     gains = []
     for j, peer in enumerate((to_x, to_y)):
         for i, ref in enumerate((ng, nb)):
-            gains.append(remote(ref, gb.at[j, i], gb_s.at[j, i], gb_r.at[j, i], peer))
+            gains.append(remote(ref, gb.at[j, i], gb_s.at[0], gb_r.at[0], peer))
     for copy in gains:
         copy.start()
 
@@ -378,8 +378,7 @@
     for j in range(G):
         ms[pl.ds(j * part, part), :] = get_stats(st, j * part, part)
     spread_own(3)
-    for copy in gains:
-        copy.wait_recv()
+    remote(gb, gb, gb_s.at[0], gb_r.at[0], to_x).wait_recv()
 
     def cast_d(t, carry):
         slot = lax.rem(t, 2)
@@ -434,10 +433,10 @@
                     else block(side, 1 - who, half // 2, half // 2)
                 )
                 hcopy[m, s] = [
-                    remote(own, own, h_s.at[s, 0], h_r.at[2 * s, m], to_x),
-                    remote(own, own, h_s.at[s, 1], h_r.at[2 * s + 1, m], to_y),
-                    remote(of_x, of_x, h_s.at[s, 2], h_r.at[4, m], to_y),
-                    remote(of_y, of_y, h_s.at[s, 3], h_r.at[4, m], to_x),
+                    remote(own, own, h_s.at[s, 0], h_r.at[0, m], to_x),
+                    remote(own, own, h_s.at[s, 1], h_r.at[1, m], to_y),
+                    remote(of_x, of_x, h_s.at[s, 2], h_r.at[2, m], to_y),
+                    remote(of_y, of_y, h_s.at[s, 3], h_r.at[2, m], to_x),
                 ]
 
     def scale_row(ref, s, t, who):
@@ -479,11 +478,12 @@
             hcopy[m, s][1].start()
 
     def s3(m):
-        for s in range(2):
-            hcopy[m, s][0].wait_recv()
-            hcopy[m, s][2].start()
-            hcopy[m, s][1].wait_recv()
-            hcopy[m, s][3].start()
+        (_, wid_a), (_, wid_b) = tiles[m % nt]
+        ref = hid.at[pl.ds(0, half), pl.ds(0, wid_a + wid_b)]
+        for i in range(2):
+            remote(ref, ref, h_s.at[0, i], h_r.at[i, m], to_x).wait_recv()
+            for s in range(2):
+                hcopy[m, s][2 + i].start()
 
     def out_cols(n):
         return pl.ds(pl.multiple_of(n * TILE, TILE), TILE)
@@ -506,7 +506,7 @@
     def relays_in(m):
         (_, wid_a), (_, wid_b) = tiles[m % nt]
         ref = hid.at[pl.ds(0, half), pl.ds(0, wid_a + wid_b)]
-        remote(ref, ref, h_s.at[0, 2], h_r.at[4, m], to_x).wait_recv()
+        remote(ref, ref, h_s.at[0, 2], h_r.at[2, m], to_x).wait_recv()
 
     nn = width // TILE
 
@@ -671,8 +671,9 @@
     swap2 = swap_stats(st2, 1)
     for copy in swap2:
         copy.start()
-    for copy in swap1 + gains:
+    for copy in swap1:
         copy.wait_send()
+    remote(gb, gb, gb_s.at[0], gb_r.at[0], to_x).wait_send()
     for k in range(G - 1):
         remote(bp.at[k], bp.at[k], bp_s.at[k], bp_r.at[0, 0], to_x).wait_send()
     for j in range(2):
@@ -685,7 +686,7 @@
         remote(away, away, c_s.at[s], c_r.at[s, 0], to_x).wait_send()
         for i in range(4):
             ref = away.at[0] if i < 2 else away.at[0, pl.ds(0, rows // 4)]
-            remote(ref, ref, h_s.at[s, i], h_r.at[4, 0], to_x).wait_send()
+            remote(ref, ref, h_s.at[s, i], h_r.at[2, 0], to_x).wait_send()
     for way in range(2):
         for dist in range(G - 1):
 
@@ -779,8 +780,8 @@
             dma((2, PIECES)),
             dma((2, G - 1)),
             dma((2, G - 1, PIECES)),
-            dma((2, 2)),
-            dma((2, 2)),
+            dma((1,)),
+            dma((1,)),
             dma((2,)),
             dma((nt, 2)),
             dma((2,)),
@@ -788,7 +789,7 @@
             dma((2,)),
             dma((2, steps)),
             dma((2, 4)),
-            dma((5, steps)),
+            dma((3, steps)),
             dma((G - 1,)),
             dma((2, width // TILE)),
             dma((2, width // TILE)),

time: 138 us -> 138 us (level)
  no operation moved by 1% of the time
where the time goes in v5:
time: 138 us
  Pallas kernels  137 us (99%)
    pallas_call x1, Pallas kernels, fused(): pl.pallas_call(kernel, out_shape=pltpu.VMEM((part, width), BF16), in_spec...  137 us

profile of v5, /device:TPU:0, one launch (start us, length us, event | category | flops | bytes accessed | tf_op | source)
XLA Modules:
  0.0 137.7 jit_solution(4962916516258817172)
XLA Ops:
  0.0 136.9 %shard_map.109 = bf16[256,1024]{1,0:T(8,128)(2,1)S(1)} custom-call(bf16[1024,1024]{1,0:T(8,128)(2,1)} %tok_hbm.1, f32[1,1024]{1,0:T(1,128)} %bitcast.9, f32[1,1024]{1,0:T(1,128)} %bitcast.10, f32[1024,2816]{1,0:T(8,128)} %gw.1, f32[1024,2816]{1,0:T(8,128)} %uw.1, f32[22,128]{1,0:T(8,128)} %bitcast.7, f32[22,128]{1,0:T(8,128)} %bitcast.8, f32[2816,1024]{1,0:T(8,128)} %dw.1, ...), custom_call_target="tpu_custom_call" | custom-call | tf_op jit(solution)/shard_map/pallas_call | solution.py:737
  136.9 0.8 copy.13
